TPU v7x, 32 devices: a whole 2x2x4 slice. The times are simulated.
32 devices in a mesh: sp: 8 (over z, x), tp: 4 (over y, core).
Axes of the slice: x: 2, y: 2, z: 4, core: 2. Of those that a mesh axis runs over, the one named last changes fastest.
Arguments:
- tokens: bfloat16 [1024, 2048], P('sp'), may hold values from -6 to 6
- pre_gain: float32 [2048], replicated, may hold values from 0.1 to 1.9
- outer_gate: bfloat16 [2048, 1024], P('sp', 'tp'), may hold values from -0.125 to 0.125
- inner_gate: bfloat16 [2048, 1024], P('sp', 'tp'), may hold values from -0.125 to 0.125
- conv_input: bfloat16 [2048, 1024], P('sp', 'tp'), may hold values from -0.125 to 0.125
- conv_taps: float32 [3, 1024], P(None, 'tp'), may hold values from -3.5 to 3.5
- query_down: bfloat16 [2048, 768], P(None, 'tp'), may hold values from -0.088388348 to 0.088388348
- latent_down: bfloat16 [2048, 512], P(None, 'tp'), may hold values from -0.088388348 to 0.088388348
- rotary_down: bfloat16 [2048, 32], replicated, may hold values from -0.125 to 0.125
- query_gain: float32 [768], replicated, may hold values from 1 to 3
- latent_gain: float32 [512], replicated, may hold values from 1 to 3
- query_up: bfloat16 [768, 512], P(None, 'tp'), may hold values from -0.14433757 to 0.14433757
- query_rotary: bfloat16 [768, 256], P(None, 'tp'), may hold values from -0.21875 to 0.21875
- key_up: bfloat16 [512, 512], P(None, 'tp'), may hold values from -4.33012702 to 4.33012702
- value_up: bfloat16 [512, 512], P(None, 'tp'), may hold values from -0.25 to 0.25
- conv_output: bfloat16 [1024, 2048], P('tp'), may hold values from -0.15625 to 0.15625
- heads_output: bfloat16 [512, 2048], P('tp'), may hold values from -0.15625 to 0.15625
- post_gain: float32 [2048], replicated, may hold values from 0.1 to 1.9
Outputs:
- mixed: bfloat16 [1024, 2048], P(('sp', 'tp'))
- row_logsum: float32 [8, 1024], P('tp', 'sp')
All inputs are finite; a program needn't handle non-finite values.
Results may differ from a plain program's by a relative error of at most 0.013.
Values may be sent and summed in bfloat16 or wider, within the bound.
A program may use at most 64 MiB of HBM per device.

v0:
```python
import math

import jax
import jax.numpy as jnp
from jax import lax
from jax.sharding import PartitionSpec as P

NOPE = 64
ROPE = 32
VDIM = 64
TAPS = 3


eps = 1e-06
rope_theta = 500000.0


def shifted(value, axis, steps):
    count = lax.axis_size(axis)
    first, last = (max(0, -steps), min(count, count - steps))
    return lax.ppermute(value, axis, [(source, source + steps) for source in range(first, last)])


def rms_scale(values, scale_row):
    widened = values.astype(jnp.float32)
    return (
        widened * lax.rsqrt(jnp.mean(widened * widened, axis=-1, keepdims=True) + eps) * scale_row
    )


def rotate(values, positions):
    half_width = values.shape[-1] // 2
    frequency = rope_theta ** (-jnp.arange(half_width, dtype=jnp.float32) / half_width)
    angles = positions.astype(jnp.float32)[:, None] * frequency
    cosine = jnp.cos(angles)[:, None, :]
    sine_part = jnp.sin(angles)[:, None, :]
    leading = values[..., :half_width]
    trailing = values[..., half_width:]
    return jnp.concatenate(
        [leading * cosine - trailing * sine_part, trailing * cosine + leading * sine_part], axis=-1
    )


def attend(
    state_now, query_nope, query_turned, key_nope, key_rotary, value_rows, key_first, query_position
):
    row_best, weight_sum, weighted = state_now
    heads_here = query_nope.shape[1]
    key_count = key_nope.shape[0]
    key_heads = key_nope.reshape(key_count, heads_here, NOPE)
    value_heads = value_rows.reshape(key_count, heads_here, VDIM)
    scores = jnp.einsum("qhd,khd->hqk", query_nope, key_heads, preferred_element_type=jnp.float32)
    scores = scores + jnp.einsum(
        "qhd,kd->hqk", query_turned, key_rotary, preferred_element_type=jnp.float32
    )
    scores = scores * (NOPE + ROPE) ** (-0.5)
    key_position = key_first + jnp.arange(key_count, dtype=jnp.int32)
    causal = key_position[None, :] <= query_position[:, None]
    scores = jnp.where(causal[None], scores, -1e30)
    new_best = jnp.maximum(row_best, jnp.max(scores, axis=-1))
    weights = jnp.where(causal[None], jnp.exp(scores - new_best[..., None]), 0.0)
    shrink = jnp.exp(row_best - new_best)
    weight_sum = weight_sum * shrink + jnp.sum(weights, axis=-1)
    weighted = weighted * shrink[..., None] + jnp.einsum(
        "hqk,khd->hqd",
        weights.astype(jnp.bfloat16),
        value_heads,
        preferred_element_type=jnp.float32,
    )
    return (new_best, weight_sum, weighted)


def fold_blocks(state_now, pieces, key_first, step_rule):
    total_rows = pieces[0].shape[0]
    if total_rows <= 1024:
        return step_rule(state_now, pieces, key_first)
    block_width = math.gcd(total_rows, 1024)
    block_count = total_rows // block_width
    stacked = tuple(
        (member.reshape(block_count, block_width, member.shape[1]) for member in pieces)
    )

    def one_block(state_in, inputs):
        block_index, block_pieces = inputs
        return (step_rule(state_in, block_pieces, key_first + block_index * block_width), None)

    state_out, unused = lax.scan(
        one_block, state_now, (jnp.arange(block_count, dtype=jnp.int32), stacked)
    )
    return state_out


def local(
    tokens,
    pre_gain,
    outer_gate,
    inner_gate,
    conv_input,
    conv_taps,
    query_down,
    latent_down,
    rotary_down,
    query_gain,
    latent_gain,
    query_up,
    query_rotary,
    key_up,
    value_up,
    conv_output,
    heads_output,
    post_gain,
):
    row_count = tokens.shape[0]
    normed = rms_scale(tokens, pre_gain).astype(jnp.bfloat16)
    sp_index = lax.axis_index("sp")
    positions = sp_index * row_count + jnp.arange(row_count, dtype=jnp.int32)
    pieces = (
        lax.all_gather(outer_gate, "sp", axis=0, tiled=True),
        lax.all_gather(inner_gate, "sp", axis=0, tiled=True),
        lax.all_gather(conv_input, "sp", axis=0, tiled=True),
    )
    outer_part, inner_part, signal = tuple(
        (jnp.dot(normed, member, preferred_element_type=jnp.float32) for member in pieces)
    )
    product = (inner_part * signal).astype(jnp.bfloat16)
    edge_rows = shifted(product[row_count - (TAPS - 1) :], "sp", 1)
    extended = jnp.concatenate([edge_rows, product], axis=0).astype(jnp.float32)
    convolved = extended[0:row_count] * conv_taps[0]
    for offset in range(1, TAPS):
        convolved = convolved + extended[offset : offset + row_count] * conv_taps[offset]
    conv_mixed = (outer_part * convolved).astype(jnp.bfloat16)
    query_latent = jnp.dot(normed, query_down, preferred_element_type=jnp.float32).astype(
        jnp.bfloat16
    )
    key_latent = jnp.dot(normed, latent_down, preferred_element_type=jnp.float32).astype(
        jnp.bfloat16
    )
    query_latent, key_latent = (
        lax.all_gather(query_latent, "tp", axis=1, tiled=True),
        lax.all_gather(key_latent, "tp", axis=1, tiled=True),
    )
    query_normed = rms_scale(query_latent, query_gain).astype(jnp.bfloat16)
    latent_normed = rms_scale(key_latent, latent_gain).astype(jnp.bfloat16)
    rotary_raw = jnp.dot(normed, rotary_down, preferred_element_type=jnp.float32)
    key_rotary = rotate(rotary_raw[:, None, :], positions)[:, 0, :].astype(jnp.bfloat16)
    heads_here = query_up.shape[1] // NOPE
    query_nope = jnp.dot(query_normed, query_up, preferred_element_type=jnp.float32).astype(
        jnp.bfloat16
    )
    query_nope = query_nope.reshape(row_count, heads_here, NOPE)
    turned_raw = jnp.dot(query_normed, query_rotary, preferred_element_type=jnp.float32)
    query_turned = rotate(turned_raw.reshape(row_count, heads_here, ROPE), positions).astype(
        jnp.bfloat16
    )
    key_nope = jnp.dot(latent_normed, key_up, preferred_element_type=jnp.float32).astype(
        jnp.bfloat16
    )
    value_rows = jnp.dot(latent_normed, value_up, preferred_element_type=jnp.float32).astype(
        jnp.bfloat16
    )
    initial = (
        jnp.full((heads_here, row_count), -1e30, jnp.float32),
        jnp.zeros((heads_here, row_count), jnp.float32),
        jnp.zeros((heads_here, row_count, VDIM), jnp.float32),
    )

    def heads_step(state_now, block_pieces, key_first):
        return attend(
            state_now,
            query_nope,
            query_turned,
            block_pieces[0],
            block_pieces[1],
            block_pieces[2],
            key_first,
            positions,
        )

    row_best, weight_sum, weighted = fold_blocks(
        initial,
        (
            lax.all_gather(key_nope, "sp", axis=0, tiled=True),
            lax.all_gather(key_rotary, "sp", axis=0, tiled=True),
            lax.all_gather(value_rows, "sp", axis=0, tiled=True),
        ),
        jnp.int32(0),
        heads_step,
    )
    heads_mixed = (weighted / weight_sum[..., None]).astype(jnp.bfloat16)
    heads_mixed = heads_mixed.transpose(1, 0, 2).reshape(row_count, heads_here * VDIM)
    row_logsum = row_best + jnp.log(weight_sum)
    projected = lax.psum_scatter(
        (
            jnp.dot(conv_mixed, conv_output, preferred_element_type=jnp.float32)
            + jnp.dot(heads_mixed, heads_output, preferred_element_type=jnp.float32)
        ).astype(jnp.bfloat16),
        "tp",
        scatter_dimension=0,
        tiled=True,
    ).astype(jnp.float32)
    mixed = rms_scale(projected, post_gain).astype(jnp.bfloat16)
    return (mixed, row_logsum)


def solution(mesh):
    in_specs = (
        P("sp", None),
        P(),
        P("sp", "tp"),
        P("sp", "tp"),
        P("sp", "tp"),
        P(None, "tp"),
        P(None, "tp"),
        P(None, "tp"),
        P(),
        P(),
        P(),
        P(None, "tp"),
        P(None, "tp"),
        P(None, "tp"),
        P(None, "tp"),
        P("tp", None),
        P("tp", None),
        P(),
    )
    out_specs = (P(("sp", "tp"), None), P("tp", "sp"))
    return jax.shard_map(local, mesh=mesh, in_specs=in_specs, out_specs=out_specs, check_vma=False)
```

profile of v0, /device:TPU:27, one launch (start us, length us, event | category | flops | bytes accessed | tf_op | source)
XLA Modules:
  0.0 168.0 jit_solution(11511326785500772555)
XLA Ops:
  7.2 0.7 all-gather.7.cloned.1.call-update
  8.0 0.7 all-gather.9.cloned.1.call-update
  8.7 0.7 all-gather.5.cloned.1.call-update
  9.5 1.2 fusion.10
  10.8 1.4 convolution_convert_fusion.3
  12.3 6.1 %all_gather.28 = bf16[128,512]{1,0:T(8,128)(2,1)S(1)} all-gather(bf16[128,128]{1,0:T(8,128)(2,1)S(1)} %convolution_convert_fusion.3), channel_id=1, replica_groups=mesh['sp'=8,'tp'=4] {'tp'}, dimensions={1}, use_global_device_ids=true | all-gather | bytes 163840 | tf_op jit(solution)/shard_map/all_gather | solution.py:140
  18.7 25.2 %all_gather.29 = bf16[1024,128]{1,0:T(8,128)(2,1)S(1)} all-gather(bf16[128,128]{1,0:T(8,128)(2,1)S(1)} %convolution_convert_fusion.2), channel_id=1, replica_groups=mesh['sp'=8,'tp'=4] {'sp'}, dimensions={0}, use_global_device_ids=true | all-gather | bytes 294912 | tf_op jit(solution)/shard_map/all_gather | solution.py:182
  44.6 11.7 %all_gather.27 = bf16[128,768]{0,1:T(8,128)(2,1)S(1)} all-gather(bf16[128,192]{0,1:T(8,128)(2,1)S(1)} %convolution_convert_fusion), channel_id=1, replica_groups=mesh['sp'=8,'tp'=4] {'tp'}, dimensions={1}, use_global_device_ids=true | all-gather | bytes 245760 | tf_op jit(solution)/shard_map/all_gather | solution.py:139
  56.4 0.6 copy-done.13
  58.2 0.6 copy-done.10
  59.4 20.8 %all-gather = bf16[1024,1,32]{0,2,1:T(8,128)(2,1)S(1)} all-gather(bf16[128,1,32]{0,2,1:T(8,128)(2,1)S(1)} %pad_maximum_fusion), channel_id=2, replica_groups=mesh['sp'=8,'tp'=4] {'sp'}, dimensions={0}, use_global_device_ids=true | all-gather | bytes 73728 | tf_op jit(solution)/shard_map/all_gather | solution.py:183
  80.7 0.5 fusion.65
  81.9 24.9 %all_gather.31 = bf16[1024,128]{1,0:T(8,128)(2,1)S(1)} all-gather(bf16[128,128]{1,0:T(8,128)(2,1)S(1)} %convolution_convert_fusion.1), channel_id=1, replica_groups=mesh['sp'=8,'tp'=4] {'sp'}, dimensions={0}, use_global_device_ids=true | all-gather | bytes 294912 | tf_op jit(solution)/shard_map/all_gather | solution.py:184
  107.3 0.6 log_add_fusion
  108.4 1.6 fusion.60
  110.0 1.6 fusion.5
  111.6 1.3 collective-permute-start
  112.9 3.3 %collective-permute-done = bf16[2,256]{1,0:T(2,128)(2,1)S(1)} collective-permute-done((bf16[2,256]{1,0:T(2,128)(2,1)S(1)}, bf16[2,256]{1,0:T(2,128)(2,1)S(1)}, u32[]{:S(2)}, u32[]{:S(2)}) %collective-permute-start) | collective-permute-done | bytes 1056 | tf_op jit(solution)/shard_map/ppermute | solution.py:21
  116.2 15.6 %all-gather.5.cloned.1.call-done = bf16[2048,256]{1,0:T(8,128)(2,1)} async-done(((bf16[256,256]{1,0:T(8,128)(2,1)}), bf16[2048,256]{1,0:T(8,128)(2,1)}) %all-gather.5.cloned.1.call-update) | async-done | bytes 1048592 | tf_op jit(solution)/shard_map/all_gather | solution.py:118
  131.8 2.1 %fusion.6 = f32[128,2048]{1,0:T(8,128)S(1)} fusion(bf16[256,2048]{1,0:T(8,128)(2,1)S(1)} %copy-done, bf16[2048,256]{1,0:T(8,128)(2,1)} %all-gather.5.cloned.1.call-done, f32[130,256]{1,0:T(8,128)S(1)} %maximum_convert_fusion, f32[256]{0:T(256)S(1)} %bitcast.60, f32[256]{0:T(256)S(1)} %bitcast.61, f32[256]{0:T(256)S(1)} %bitcast.59, ...), kind=kOutput, calls=%fused_computation.13 | convolution fusion | flops 269713408 | bytes 4075008 | tf_op jit(solution)/shard_map/dot_general | solution.py:194
  133.9 1.1 fusion
  135.1 24.5 %reduce-scatter.2.cloned.1.call-done = bf16[32,2048]{1,0:T(8,128)(2,1)} async-done(((bf16[128,2048]{1,0:T(8,128)(2,1)}), bf16[32,2048]{1,0:T(8,128)(2,1)}) %reduce-scatter.2.cloned.1.call-update) | async-done | bytes 131088 | tf_op jit(solution)/shard_map/reduce_scatter | solution.py:192
  159.6 1.1 fusion.25
  160.7 0.8 fusion.27
  (65 shorter events, 5.3 us)
Async XLA Ops:
  7.2 124.7 %copy-start = (bf16[256,2048]{1,0:T(8,128)(2,1)S(1)}, bf16[256,2048]{1,0:T(8,128)(2,1)}, u32[]{:S(2)}) copy-start(bf16[256,2048]{1,0:T(8,128)(2,1)} %param.33) | copy-start | bytes 3145732
  7.2 3.6 %copy-start.1 = (bf16[128,2048]{1,0:T(8,128)(2,1)S(1)}, bf16[128,2048]{1,0:T(8,128)(2,1)}, u32[]{:S(2)}) copy-start(bf16[128,2048]{1,0:T(8,128)(2,1)} %param.18) | copy-start | bytes 1572868
  7.2 101.2 %all-gather.7.cloned.1.call-start = ((), (), s32[]{:S(2)}) async-start(), calls=%async_computation.2 | async-start | bytes 1179648 | tf_op jit(solution)/shard_map/all_gather | solution.py:119
  7.9 102.0 %all-gather.9.cloned.1.call-start = ((), (), s32[]{:S(2)}) async-start(), calls=%async_computation.3 | async-start | bytes 1179648 | tf_op jit(solution)/shard_map/all_gather | solution.py:120
  8.7 123.2 %all-gather.5.cloned.1.call-start = ((), (), s32[]{:S(2)}) async-start(), calls=%async_computation.1 | async-start | bytes 1179648 | tf_op jit(solution)/shard_map/all_gather | solution.py:118
  9.4 150.2 %reduce-scatter.2.cloned.1.call-start = ((), (), s32[]{:S(2)}) async-start(), calls=%async_computation.4 | async-start | bytes 655360 | tf_op jit(solution)/shard_map/reduce_scatter | solution.py:192
  9.5 1.3 copy-start.4
  10.8 7.7 %copy-start.9 = (bf16[512,128]{1,0:T(8,128)(2,1)S(1)}, bf16[512,128]{1,0:T(8,128)(2,1)}, u32[]{:S(2)}) copy-start(bf16[512,128]{1,0:T(8,128)(2,1)} %param.31) | copy-start | bytes 393220
  10.8 7.7 %copy-start.14 = (f32[512]{0:T(512)S(1)}, f32[512]{0:T(512)}, u32[]{:S(2)}) copy-start(f32[512]{0:T(512)} %param.28) | copy-start | bytes 6148
  12.2 31.8 %copy-start.7 = (bf16[2048,192]{0,1:T(8,128)(2,1)S(1)}, bf16[2048,192]{0,1:T(8,128)(2,1)}, u32[]{:S(2)}) copy-start(bf16[2048,192]{0,1:T(8,128)(2,1)} %param.24) | copy-start | bytes 2359300
  44.6 11.9 %copy-start.8 = (bf16[768,128]{1,0:T(8,128)(2,1)S(1)}, bf16[768,128]{1,0:T(8,128)(2,1)}, u32[]{:S(2)}) copy-start(bf16[768,128]{1,0:T(8,128)(2,1)} %param.29) | copy-start | bytes 589828
  56.3 0.7 copy-start.13
  57.0 0.9 copy-start.12
  57.9 0.9 copy-start.10
  80.7 0.9 copy-start.11
  110.0 2.9 %copy-start.6 = (f32[3,256]{1,0:T(4,128)S(1)}, f32[3,256]{1,0:T(4,128)}, u32[]{:S(2)}) copy-start(f32[3,256]{1,0:T(4,128)} %param.23) | copy-start | bytes 9220
  111.6 4.6 %collective-permute-start = (bf16[2,256]{1,0:T(2,128)(2,1)S(1)}, bf16[2,256]{1,0:T(2,128)(2,1)S(1)}, u32[]{:S(2)}, u32[]{:S(2)}) collective-permute-start(bf16[2,256]{1,0:T(2,128)(2,1)S(1)} %slice.44), channel_id=1, source_target_pairs={{0,4},{4,8},{8,12},{12,16},{16,20},{20,24},{24,28},{1,5},{5,9},{9,... | collective-permute-start | bytes 3080 | tf_op jit(solution)/shard_map/ppermute | solution.py:21
  131.8 2.1 %copy-start.3 = (bf16[128,2048]{1,0:T(8,128)(2,1)S(1)}, bf16[128,2048]{1,0:T(8,128)(2,1)}, u32[]{:S(2)}) copy-start(bf16[128,2048]{1,0:T(8,128)(2,1)} %param.34) | copy-start | bytes 1572868
  135.1 25.6 %copy-start.5 = (f32[2048]{0:T(1024)S(1)}, f32[2048]{0:T(1024)}, u32[]{:S(2)}) copy-start(f32[2048]{0:T(1024)} %param.35) | copy-start | bytes 24580
  159.6 1.1 copy-start.2
Sparse Core Ops, SparseCore 0:
  10.1 38.6 all-gather.6
  51.0 39.2 all-gather.8
  92.4 39.3 all-gather.4
  135.2 24.3 reduce-scatter.1
where the time goes:
time: 170 us; the launch traced here: 168 us
  blocking collectives  88.7 us (52%)
  waiting for transfers between devices  45.5 us (27%)
  between operations  14.1 us (8%)
  matrix products  11.1 us (7%)
  other arithmetic  4.76 us (3%)
  local copies, waits for them, and re-layouts  2.4 us (1%)
    all_gather x1, blocking collectives, local(): lax.all_gather(key_nope, 'sp', axis=0, tiled=True)  25.2 us
    all_gather x1, blocking collectives, local(): lax.all_gather(value_rows, 'sp', axis=0, tiled=True)  24.9 us
    reduce_scatter x1, waiting for transfers between devices, local(): lax.psum_scatter((jnp.dot(conv_mixed, conv_output, preferred_element_type...  24.5 us
    all_gather x1, blocking collectives, local(): lax.all_gather(key_rotary, 'sp', axis=0, tiled=True)  20.8 us
    all_gather x1, waiting for transfers between devices, local(): lax.all_gather(outer_gate, 'sp', axis=0, tiled=True)  15.6 us
    all_gather x1, blocking collectives, local(): lax.all_gather(query_latent, 'tp', axis=1, tiled=True)  11.7 us
    all_gather x1, blocking collectives, local(): lax.all_gather(key_latent, 'tp', axis=1, tiled=True)  6.09 us
  transfers between devices with their start and end apart: 5, of which 3 were waited for; matrix products, arithmetic and copies ran while one was open for 7% of the time, Pallas kernels for 0%

commit v1 on v0

v1 whole, which is shorter than its diff:
```python
import functools

import jax
import jax.numpy as jnp
import numpy as np
from jax import lax
from jax.experimental import pallas as pl
from jax.experimental.pallas import tpu as pltpu
from jax.sharding import PartitionSpec as P

NOPE = 64
ROPE = 32
VDIM = 64
TAPS = 3
HALO = 16

eps = 1e-06
rope_theta = 500000.0
F32 = jnp.float32
BF16 = jnp.bfloat16
MESH = pl.DeviceIdType.MESH


def dot(a, b):
    return jnp.dot(a, b, preferred_element_type=F32)


def dot_nt(a, b):
    return lax.dot_general(a, b, (((1,), (1,)), ((), ())), preferred_element_type=F32)


def normalized(values, gain):
    wide = values.astype(F32)
    return wide * lax.rsqrt(jnp.mean(wide * wide, axis=-1, keepdims=True) + eps) * gain


def swapped(values):
    half = ROPE // 2
    parts = []
    for first in range(0, values.shape[-1], ROPE):
        parts += [values[:, first + half : first + ROPE], values[:, first : first + half]]
    return jnp.concatenate(parts, axis=1)


def kernel(
    sp, tp, inner,
    tokens, pre_gain, outer_gate, inner_gate, conv_input, conv_taps, query_down, latent_down,
    rotary_down, query_gain, latent_gain, query_up, query_rotary, key_up, value_up,
    conv_output, heads_output, post_gain, table,
    mixed, row_logsum,
    wbuf, normed, halo, acc, prod, qlat, klat, kvbuf, qcat, best, total, weighted, proj,
    convm, outbuf, rsbuf, wout, wheads, tab,
    local_sem, w_recv, w_send, halo_sem, lat_send, lat_recv, kv_send, kv_recv, rs_send, rs_recv,
):
    rows = tokens.shape[0]
    depth = outer_gate.shape[0]
    heads = query_up.shape[1] // NOPE
    lines = sp // inner
    me = lax.axis_index("sp")
    mine = lax.axis_index("tp")
    zi = me // inner
    xi = me % inner
    ql = query_down.shape[1]
    kl = latent_down.shape[1]

    def sp_row(slot):
        return pl.ds(pl.multiple_of(slot * depth, depth), depth)

    locals_ = [
        pltpu.make_async_copy(ref, wbuf.at[i, sp_row(me)], local_sem.at[i])
        for i, ref in enumerate((outer_gate, inner_gate, conv_input))
    ]
    locals_ += [
        pltpu.make_async_copy(
            table.at[pl.ds(pl.multiple_of(me * rows, rows), rows)], tab, local_sem.at[3]
        ),
        pltpu.make_async_copy(heads_output, wheads, local_sem.at[4]),
        pltpu.make_async_copy(conv_output, wout, local_sem.at[5]),
    ]
    for copy in locals_:
        copy.start()

    barrier = pltpu.get_barrier_semaphore()

    def greet_sp(k, carry):
        pl.semaphore_signal(barrier, inc=1, device_id={"sp": (me + k) % sp}, device_id_type=MESH)
        return carry

    lax.fori_loop(1, sp, greet_sp, 0)
    for k in range(1, tp):
        pl.semaphore_signal(barrier, inc=1, device_id={"tp": (mine + k) % tp}, device_id_type=MESH)

    normed[pl.ds(HALO, rows), :] = normalized(tokens[...], pre_gain[...]).astype(BF16)
    pl.semaphore_wait(barrier, sp + tp - 2)

    def w_copy(i, slot, way):
        if way == 2:
            target = zi * inner + (inner - 1 - xi)
        else:
            target = me + (inner if way == 0 else -inner)
        return pltpu.make_async_remote_copy(
            src_ref=wbuf.at[i, sp_row(slot)],
            dst_ref=wbuf.at[i, sp_row(slot)],
            send_sem=w_send.at[way, i, slot],
            recv_sem=w_recv.at[i, slot],
            device_id={"sp": target},
            device_id_type=MESH,
        )

    def w_wait(i, slot):
        pltpu.make_async_copy(
            wbuf.at[i, sp_row(slot)], wbuf.at[i, sp_row(slot)], w_recv.at[i, slot]
        ).wait()

    halo_copy = pltpu.make_async_remote_copy(
        src_ref=tokens.at[pl.ds(rows - HALO, HALO)],
        dst_ref=halo,
        send_sem=halo_sem.at[0],
        recv_sem=halo_sem.at[1],
        device_id={"sp": (me + 1) % sp},
        device_id_type=MESH,
    )

    @pl.when(me < sp - 1)
    def _():
        halo_copy.start()

    for i in range(3):
        locals_[i].wait()

        @pl.when(zi < lines - 1)
        def _():
            w_copy(i, me, 0).start()

        @pl.when(zi > 0)
        def _():
            w_copy(i, me, 1).start()

        w_copy(i, me, 2).start()

    own = normed[pl.ds(HALO, rows), :]
    klat[mine] = dot(own, latent_down[...]).astype(BF16)
    qlat[mine] = dot(own, query_down[...]).astype(BF16)

    def lat_copy(which, k):
        buf = (klat, qlat)[which]
        return pltpu.make_async_remote_copy(
            src_ref=buf.at[mine],
            dst_ref=buf.at[mine],
            send_sem=lat_send.at[which, k],
            recv_sem=lat_recv.at[which, mine],
            device_id={"tp": (mine + k) % tp},
            device_id_type=MESH,
        )

    for which in range(2):
        for k in range(1, tp):
            lat_copy(which, k).start()

    rotary_raw = dot(own, rotary_down[...])

    @pl.when(me == 0)
    def _():
        normed[pl.ds(0, HALO), :] = jnp.zeros((HALO, normed.shape[1]), BF16)

    @pl.when(me > 0)
    def _():
        halo_copy.wait_recv()
        normed[pl.ds(0, HALO), :] = normalized(halo[...], pre_gain[...]).astype(BF16)

    locals_[3].wait()
    width = heads * ROPE
    cosine, sine = tab[:, :width], tab[:, width : 2 * width]
    key_rotary = (
        rotary_raw * cosine[:, :ROPE] + swapped(rotary_raw) * sine[:, :ROPE]
    ).astype(BF16)

    def lat_wait(which):
        buf = (klat, qlat)[which]
        for k in range(1, tp):
            other = (mine + k) % tp
            pltpu.make_async_copy(buf.at[other], buf.at[other], lat_recv.at[which, other]).wait()

    lat_wait(0)
    latent = jnp.concatenate([klat[t] for t in range(tp)], axis=1)
    latent_normed = normalized(latent, latent_gain[...]).astype(BF16)
    key_nope = dot(latent_normed, key_up[...]).astype(BF16)
    values = dot(latent_normed, value_up[...]).astype(BF16)
    tail = kvbuf.shape[3] - NOPE - ROPE
    blank = [jnp.zeros((rows, tail), BF16)] if tail else []
    for h in range(heads):
        kvbuf[me, h] = jnp.concatenate(
            [key_nope[:, h * NOPE : (h + 1) * NOPE], key_rotary] + blank, axis=1
        )
    kvbuf[me, heads] = values

    def kv_copy(target):
        return pltpu.make_async_remote_copy(
            src_ref=kvbuf.at[me],
            dst_ref=kvbuf.at[me],
            send_sem=kv_send.at[target],
            recv_sem=kv_recv.at[me],
            device_id={"sp": target},
            device_id_type=MESH,
        )

    def kv_start(target, carry):
        kv_copy(target).start()
        return carry

    lax.fori_loop(me + 1, sp, kv_start, 0)

    lat_wait(1)
    wide = [qlat[t].astype(F32) for t in range(tp)]
    squares = sum(jnp.sum(w * w, axis=-1, keepdims=True) for w in wide)
    scale = lax.rsqrt(squares / (ql * tp) + eps)
    query_nope = jnp.zeros((rows, heads * NOPE), F32)
    turned = jnp.zeros((rows, width), F32)
    for t in range(tp):
        piece = (wide[t] * scale * query_gain[t : t + 1, :]).astype(BF16)
        query_nope = query_nope + dot(piece, query_up[t * ql : (t + 1) * ql, :])
        turned = turned + dot(piece, query_rotary[t * ql : (t + 1) * ql, :])
    query_nope = query_nope.astype(BF16)
    turned = (turned * cosine + swapped(turned) * sine).astype(BF16)
    for h in range(heads):
        qcat[h] = jnp.concatenate(
            [
                query_nope[:, h * NOPE : (h + 1) * NOPE],
                turned[:, h * ROPE : (h + 1) * ROPE],
            ]
            + blank,
            axis=1,
        )

    aligned = depth % 128 == 0

    def gate_step(i, slot, first=False):
        columns = pl.ds(pl.multiple_of(slot * depth, depth), depth)
        value = dot(normed[:, columns], wbuf[i, sp_row(slot), :])
        if first:
            acc[i] = value
        else:
            acc[i] += value

    if aligned:
        for i in range(3):
            gate_step(i, me, True)

    def line_step(d, carry):
        for i in range(3):

            @pl.when(zi - d >= 0)
            def _():
                slot = me - d * inner
                w_wait(i, slot)

                @pl.when(zi < lines - 1)
                def _():
                    w_copy(i, slot, 0).start()

                w_copy(i, slot, 2).start()

            @pl.when(zi + d <= lines - 1)
            def _():
                slot = me + d * inner
                w_wait(i, slot)

                @pl.when(zi > 0)
                def _():
                    w_copy(i, slot, 1).start()

                w_copy(i, slot, 2).start()

        if aligned:

            @pl.when(zi - d >= 0)
            def _():
                for i in range(3):
                    gate_step(i, me - d * inner)

            @pl.when(zi + d <= lines - 1)
            def _():
                for i in range(3):
                    gate_step(i, me + d * inner)

        return carry

    lax.fori_loop(1, lines, line_step, 0)

    factor = (NOPE + ROPE) ** (-0.5)
    row_id = lax.broadcasted_iota(jnp.int32, (rows, rows), 0)
    key_id = lax.broadcasted_iota(jnp.int32, (rows, rows), 1)
    for h in range(heads):
        scores = dot_nt(qcat[h], kvbuf[me, h]) * factor
        scores = jnp.where(key_id <= row_id, scores, -1e30)
        top = jnp.max(scores, axis=-1, keepdims=True)
        weights = jnp.where(key_id <= row_id, jnp.exp(scores - top), 0.0)
        best[h] = top
        total[h] = jnp.sum(weights, axis=-1, keepdims=True)
        weighted[h] = dot(weights.astype(BF16), kvbuf[me, heads])

    def attend(k, carry):
        slot = me - k
        pltpu.make_async_copy(kvbuf.at[slot], kvbuf.at[slot], kv_recv.at[slot]).wait()
        for h in range(heads):
            scores = dot_nt(qcat[h], kvbuf[slot, h]) * factor
            old = best[h]
            top = jnp.maximum(old, jnp.max(scores, axis=-1, keepdims=True))
            weights = jnp.exp(scores - top)
            shrink = jnp.exp(old - top)
            best[h] = top
            total[h] = total[h] * shrink + jnp.sum(weights, axis=-1, keepdims=True)
            weighted[h] = weighted[h] * shrink + dot(weights.astype(BF16), kvbuf[slot, heads])
        return carry

    lax.fori_loop(1, me + 1, attend, 0)
    lane = lax.broadcasted_iota(jnp.int32, (rows, heads * VDIM), 1)
    heads_mixed = jnp.zeros((rows, heads * VDIM), F32)
    for h in range(heads):
        logsum = best[h] + jnp.log(total[h])
        row_logsum[h : h + 1, :] = jnp.transpose(jnp.broadcast_to(logsum, (rows, rows)))[0:1, :]
        heads_mixed = jnp.where(lane // VDIM == h, weighted[h] / total[h], heads_mixed)
    locals_[4].wait()
    proj[...] = dot(heads_mixed.astype(BF16), wheads[...])

    other_x = inner - 1 - xi

    def pair_slot(slot):
        for i in range(3):
            w_wait(i, slot)
            if aligned:
                gate_step(i, slot)

    pair_slot(zi * inner + other_x)

    def pair_step(d, carry):
        @pl.when(zi - d >= 0)
        def _():
            pair_slot((zi - d) * inner + other_x)

        @pl.when(zi + d <= lines - 1)
        def _():
            pair_slot((zi + d) * inner + other_x)

        return carry

    lax.fori_loop(1, lines, pair_step, 0)
    if not aligned:
        for i in range(3):
            acc[i] = dot(normed[...], wbuf[i])

    prod[...] = (acc[1] * acc[2]).astype(BF16).astype(F32)
    convolved = prod[pl.ds(HALO - TAPS + 1, rows), :] * conv_taps[0:1, :]
    for k in range(1, TAPS):
        convolved = convolved + prod[pl.ds(HALO - TAPS + 1 + k, rows), :] * conv_taps[k : k + 1, :]
    convm[...] = (acc[0, pl.ds(HALO, rows), :] * convolved).astype(BF16)

    locals_[5].wait()
    part = rows // tp

    def share(target):
        where = pl.ds(pl.multiple_of(target * part, part), part)
        return proj[where, :] + dot(convm[where, :], wout[...])

    def rs_copy(k):
        return pltpu.make_async_remote_copy(
            src_ref=outbuf.at[k],
            dst_ref=rsbuf.at[mine],
            send_sem=rs_send.at[k],
            recv_sem=rs_recv.at[mine],
            device_id={"tp": (mine + k) % tp},
            device_id_type=MESH,
        )

    order = sorted(range(1, tp), key=lambda k: abs(k - tp // 2))
    for k in order:
        outbuf[k] = share((mine + k) % tp).astype(BF16)
        rs_copy(k).start()
    result = share(mine)
    for k in range(1, tp):
        other = (mine + k) % tp
        pltpu.make_async_copy(rsbuf.at[other], rsbuf.at[other], rs_recv.at[other]).wait()
        result = result + rsbuf[other].astype(F32)
    mixed[...] = normalized(result, post_gain[...]).astype(BF16)

    for k in range(1, tp):
        rs_copy(k).wait_send()
        for which in range(2):
            lat_copy(which, k).wait_send()

    @pl.when(me < sp - 1)
    def _():
        halo_copy.wait_send()

    def kv_end(target, carry):
        kv_copy(target).wait_send()
        return carry

    lax.fori_loop(me + 1, sp, kv_end, 0)

    def w_end(z, carry):
        slot = z * inner + xi
        for i in range(3):
            w_copy(i, slot, 2).wait_send()

            @pl.when((z <= zi) & (zi < lines - 1))
            def _():
                w_copy(i, slot, 0).wait_send()

            @pl.when((z >= zi) & (zi > 0))
            def _():
                w_copy(i, slot, 1).wait_send()

        return carry

    lax.fori_loop(0, lines, w_end, 0)


def rope_table(count, heads):
    half = ROPE // 2
    frequency = np.float32(rope_theta) ** (-np.arange(half, dtype=np.float32) / np.float32(half))
    angles = np.arange(count, dtype=np.float32)[:, None] * frequency.astype(np.float32)
    cosine, sine = np.cos(angles), np.sin(angles)
    both = [np.concatenate([cosine, cosine], 1)] * heads + [np.concatenate([-sine, sine], 1)] * heads
    return np.concatenate(both, axis=1).astype(np.float32)


def solution(mesh):
    sp, tp = mesh.shape["sp"], mesh.shape["tp"]
    inner = 2

    def local(
        tokens, pre_gain, outer_gate, inner_gate, conv_input, conv_taps, query_down, latent_down,
        rotary_down, query_gain, latent_gain, query_up, query_rotary, key_up, value_up,
        conv_output, heads_output, post_gain,
    ):
        rows, model = tokens.shape
        depth, channels = outer_gate.shape
        heads = query_up.shape[1] // NOPE
        ql, kl = query_down.shape[1], latent_down.shape[1]
        slab = max(heads * VDIM, 128)
        part = rows // tp
        table = jnp.asarray(rope_table(rows * sp, heads))
        vm = pl.BlockSpec(memory_space=pltpu.VMEM)
        hbm = pl.BlockSpec(memory_space=pl.ANY)
        dma = pltpu.SemaphoreType.DMA
        return pl.pallas_call(
            functools.partial(kernel, sp, tp, inner),
            out_shape=(
                jax.ShapeDtypeStruct((part, model), BF16),
                jax.ShapeDtypeStruct((heads, rows), F32),
            ),
            in_specs=[
                vm, vm, hbm, hbm, hbm, vm, vm, vm, vm, vm, vm, vm, vm, vm, vm, hbm, hbm, vm, hbm,
            ],
            out_specs=(vm, vm),
            scratch_shapes=[
                pltpu.VMEM((3, sp * depth, channels), BF16),
                pltpu.VMEM((rows + HALO, model), BF16),
                pltpu.VMEM((HALO, model), BF16),
                pltpu.VMEM((3, rows + HALO, channels), F32),
                pltpu.VMEM((rows + HALO, channels), F32),
                pltpu.VMEM((tp, rows, ql), BF16),
                pltpu.VMEM((tp, rows, kl), BF16),
                pltpu.VMEM((sp, heads + 1, rows, slab), BF16),
                pltpu.VMEM((heads, rows, slab), BF16),
                pltpu.VMEM((heads, rows, 1), F32),
                pltpu.VMEM((heads, rows, 1), F32),
                pltpu.VMEM((heads, rows, heads * VDIM), F32),
                pltpu.VMEM((rows, model), F32),
                pltpu.VMEM((rows, channels), BF16),
                pltpu.VMEM((tp, part, model), BF16),
                pltpu.VMEM((tp, part, model), BF16),
                pltpu.VMEM(conv_output.shape, BF16),
                pltpu.VMEM(heads_output.shape, BF16),
                pltpu.VMEM((rows, 2 * heads * ROPE), F32),
                dma((6,)),
                dma((3, sp)),
                dma((3, 3, sp)),
                dma((2,)),
                dma((2, tp)),
                dma((2, tp)),
                dma((sp,)),
                dma((sp,)),
                dma((tp,)),
                dma((tp,)),
            ],
            compiler_params=pltpu.CompilerParams(collective_id=0, has_side_effects=True),
        )(
            tokens, pre_gain.reshape(1, -1), outer_gate, inner_gate, conv_input, conv_taps,
            query_down, latent_down, rotary_down, query_gain.reshape(tp, ql),
            latent_gain.reshape(1, -1), query_up, query_rotary, key_up, value_up,
            conv_output, heads_output, post_gain.reshape(1, -1), table,
        )

    in_specs = (
        P("sp", None), P(), P("sp", "tp"), P("sp", "tp"), P("sp", "tp"), P(None, "tp"),
        P(None, "tp"), P(None, "tp"), P(), P(), P(), P(None, "tp"), P(None, "tp"),
        P(None, "tp"), P(None, "tp"), P("tp", None), P("tp", None), P(),
    )
    out_specs = (P(("sp", "tp"), None), P("tp", "sp"))
    return jax.shard_map(local, mesh=mesh, in_specs=in_specs, out_specs=out_specs, check_vma=False)
```

time: 170 us -> 72.3 us (0.43); the launches traced: 168 us -> 72.1 us
  blocking collectives: 88.7 us -> 0 us
  Pallas kernels: 0 us -> 63.1 us
  waiting for transfers between devices: 45.5 us -> 0 us
  between operations: 14.1 us -> 0.67 us
  matrix products: 11.1 us -> 0 us
  local copies, waits for them, and re-layouts: 2.4 us -> 8.38 us
  other arithmetic: 4.76 us -> 0 us
    all_gather x5 -> x0, blocking collectives: 88.7 us -> none  [the longest x1 25.2 us: local(): lax.all_gather(key_nope, 'sp', axis=0, tiled=True)]
    pallas_call x0 -> x1, Pallas kernels: none -> 63.1 us  [local(): pl.pallas_call(functools.partial(kernel, sp, tp, inner), out_shape=(jax.S...]
    reduce_scatter x1 -> x0, waiting for transfers between devices: 24.5 us -> none  [local(): lax.psum_scatter((jnp.dot(conv_mixed, conv_output, preferred_element_type...]
    all_gather x3 -> x0, waiting for transfers between devices: 15.6 us -> none  [the longest x1 15.6 us: local(): lax.all_gather(outer_gate, 'sp', axis=0, tiled=True)]
    dot_general x14 -> x0, matrix products: 11.1 us -> none  [the longest x2 3.16 us: local(): jnp.dot(normed, member, preferred_element_type=jnp.float32)]
    unnamed x30 -> x11, local copies, waits for them, and re-layouts: 2.1 us -> 7.71 us
    ppermute x1 -> x0, waiting for transfers between devices: 3.31 us -> none  [shifted(): lax.ppermute(value, axis, [(source, source + steps) for source in range(f...]
    reduce_sum x5 -> x0, other arithmetic: 2.93 us -> none  [the longest x4 2.57 us: rms_scale(): jnp.mean(widened * widened, axis=-1, keepdims=True) + eps]
  transfers between devices with their start and end apart: 5 -> 0, of which waited for: 3 -> 0; matrix products, arithmetic and copies ran while one was open for 7% -> 0% of each run, Pallas kernels for 0% -> 0%
where the time goes in v1:
time: 72.3 us; the launch traced here: 72.1 us
  Pallas kernels  63.1 us (87%)
  local copies, waits for them, and re-layouts  8.38 us (12%)
    pallas_call x1, Pallas kernels, local(): pl.pallas_call(functools.partial(kernel, sp, tp, inner), out_shape=(jax.S...  63.1 us
    unnamed x11, local copies, waits for them, and re-layouts  7.71 us

profile of v1, /device:TPU:27, one launch (start us, length us, event | category | flops | bytes accessed | tf_op | source)
XLA Modules:
  0.0 72.1 jit_solution(9568565809671384232)
XLA Ops:
  0.6 0.0 copy-start.1
  0.6 0.0 copy-start
  0.6 0.7 copy-done.1
  1.3 0.7 reshape.17.query_gain
  2.0 1.7 %copy.23.query_rotary = bf16[768,64]{1,0:T(8,128)(2,1)} copy(bf16[768,64]{0,1:T(8,128)(2,1)} %param.31) | data formatting | bytes 196608 | tf_op args[12]
  3.7 1.9 %copy.22.rotary_down = bf16[2048,32]{1,0:T(8,128)(2,1)} copy(bf16[2048,32]{0,1:T(8,128)(2,1)} %param.27) | data formatting | bytes 262144 | tf_op args[8]
  5.6 0.0 copy-done
  5.6 1.3 %copy.21.query_down = bf16[2048,192]{1,0:T(8,128)(2,1)} copy(bf16[2048,192]{0,1:T(8,128)(2,1)S(1)} %copy-done) | data formatting | bytes 1572864 | tf_op args[6]
  6.9 63.1 %shard_map.194 = (bf16[32,2048]{1,0:T(8,128)(2,1)}, f32[2,128]{1,0:T(2,128)}) custom-call(bf16[128,2048]{1,0:T(8,128)(2,1)} %tokens.1, f32[1,2048]{1,0:T(1,128)} %bitcast.3, bf16[256,256]{1,0:T(8,128)(2,1)} %outer_gate.1, bf16[256,256]{1,0:T(8,128)(2,1)} %inner_gate.1, bf16[256,256]{1,0:T(8,128)(2,1)} %conv_input.1, f32[3,256]{1,0:T(4,128)} %conv_taps.1, ...), custom_call_target="tpu_custom_call" | custom-call | tf_op jit(solution)/shard_map/pallas_call | solution.py:447
  70.0 0.0 copy-start.2
  70.0 1.6 %copy.26 = bf16[32,2048]{1,0:T(8,128)(2,1)} copy(bf16[32,2048]{1,0:T(8,128)(2,1)} %get-tuple-element.4) | data formatting | bytes 262144
  71.6 0.0 copy-done.2
  71.6 0.6 copy.27
Async XLA Ops:
  0.6 0.7 copy-start.1
  0.6 5.0 %copy-start = (bf16[2048,192]{0,1:T(8,128)(2,1)S(1)}, bf16[2048,192]{0,1:T(8,128)(2,1)}, u32[]{:S(2)}) copy-start(bf16[2048,192]{0,1:T(8,128)(2,1)} %param.25) | copy-start | bytes 2359300
  70.0 1.6 %copy-start.2 = (f32[2,128]{1,0:T(2,128)S(1)}, f32[2,128]{1,0:T(2,128)}, u32[]{:S(2)}) copy-start(f32[2,128]{1,0:T(2,128)} %get-tuple-element.5) | copy-start | bytes 3076

commit v2 on v1

v2 whole, which is shorter than its diff:
```python
import functools

import jax
import jax.numpy as jnp
import numpy as np
from jax import lax
from jax.experimental import pallas as pl
from jax.experimental.pallas import tpu as pltpu
from jax.sharding import PartitionSpec as P

NOPE = 64
ROPE = 32
VDIM = 64
TAPS = 3
HALO = 16

eps = 1e-06
rope_theta = 500000.0
F32 = jnp.float32
BF16 = jnp.bfloat16
MESH = pl.DeviceIdType.MESH


def dot(a, b):
    return jnp.dot(a, b, preferred_element_type=F32)


def dot_nt(a, b):
    return lax.dot_general(a, b, (((1,), (1,)), ((), ())), preferred_element_type=F32)


def normalized(values, gain):
    wide = values.astype(F32)
    return wide * lax.rsqrt(jnp.mean(wide * wide, axis=-1, keepdims=True) + eps) * gain


def swapped(values):
    half = ROPE // 2
    parts = []
    for first in range(0, values.shape[-1], ROPE):
        parts += [values[:, first + half : first + ROPE], values[:, first : first + half]]
    return jnp.concatenate(parts, axis=1)


def kernel(
    sp, tp, inner,
    tokens, pre_gain, outer_gate, inner_gate, conv_input, conv_taps, query_down, latent_down,
    rotary_down, query_gain, latent_gain, query_up, query_rotary, key_up, value_up,
    conv_output, heads_output, post_gain, table, key_table,
    mixed, row_logsum,
    wbuf, normed, halo, acc, prod, qlat, latbuf, qnope, qturn, best, total, weighted, proj,
    convm, outbuf, rsbuf, wout, wheads, tab, key_tab,
    local_sem, w_recv, w_send, halo_sem, q_send, q_recv, lat_send, lat_recv, sp_send,
    rs_send, rs_recv,
):
    rows = tokens.shape[0]
    depth = outer_gate.shape[0]
    heads = query_up.shape[1] // NOPE
    lines = sp // inner
    me = lax.axis_index("sp")
    mine = lax.axis_index("tp")
    zi = me // inner
    xi = me % inner
    ql = query_down.shape[0]
    channels = outer_gate.shape[1]
    units = w_units(channels)
    kl = latent_down.shape[1]

    def sp_row(slot):
        return pl.ds(pl.multiple_of(slot * depth, depth), depth)

    locals_ = [
        pltpu.make_async_copy(ref, wbuf.at[i, sp_row(me)], local_sem.at[i])
        for i, ref in enumerate((outer_gate, inner_gate, conv_input))
    ]
    locals_ += [
        pltpu.make_async_copy(table.at[me], tab, local_sem.at[3]),
        pltpu.make_async_copy(key_table.at[me], key_tab, local_sem.at[6]),
        pltpu.make_async_copy(heads_output, wheads, local_sem.at[4]),
        pltpu.make_async_copy(conv_output, wout, local_sem.at[5]),
    ]
    for copy in locals_:
        copy.start()

    barrier = pltpu.get_barrier_semaphore()

    def greet_sp(k, carry):
        pl.semaphore_signal(barrier, inc=1, device_id={"sp": (me + k) % sp}, device_id_type=MESH)
        return carry

    lax.fori_loop(1, sp, greet_sp, 0)
    for k in range(1, tp):
        pl.semaphore_signal(barrier, inc=1, device_id={"tp": (mine + k) % tp}, device_id_type=MESH)

    normed[pl.ds(HALO, rows), :] = normalized(tokens[...], pre_gain[...]).astype(BF16)
    pl.semaphore_wait(barrier, sp + tp - 2)

    def w_part(u, slot):
        i, first, size = units[u]
        return wbuf.at[i, sp_row(slot), pl.ds(first, size)]

    def w_copy(u, slot, way):
        if way == 2:
            target = zi * inner + (inner - 1 - xi)
        else:
            target = me + (inner if way == 0 else -inner)
        return pltpu.make_async_remote_copy(
            src_ref=w_part(u, slot),
            dst_ref=w_part(u, slot),
            send_sem=w_send.at[way, u, slot],
            recv_sem=w_recv.at[u, slot],
            device_id={"sp": target},
            device_id_type=MESH,
        )

    def w_wait(u, slot):
        pltpu.make_async_copy(w_part(u, slot), w_part(u, slot), w_recv.at[u, slot]).wait()

    def up(u, slot):
        @pl.when(zi < lines - 1)
        def _():
            w_copy(u, slot, 0).start()

    def down(u, slot):
        @pl.when(zi > 0)
        def _():
            w_copy(u, slot, 1).start()

    late = len(units) - 1
    pair = zi * inner + (inner - 1 - xi)

    halo_copy = pltpu.make_async_remote_copy(
        src_ref=tokens.at[pl.ds(rows - HALO, HALO)],
        dst_ref=halo,
        send_sem=halo_sem.at[0],
        recv_sem=halo_sem.at[1],
        device_id={"sp": (me + 1) % sp},
        device_id_type=MESH,
    )

    @pl.when(me < sp - 1)
    def _():
        halo_copy.start()

    for i in range(3):
        locals_[i].wait()
    w_copy(late, me, 2).start()
    for u in range(late):
        up(u, me)
        down(u, me)
        w_copy(u, me, 2).start()
    up(late, me)
    down(late, me)

    own = normed[pl.ds(HALO, rows), :]
    latbuf[me, mine, 0:rows, 0:kl] = dot(own, latent_down[...]).astype(BF16)
    key_raw = dot_nt(rotary_down[...], own)
    half = ROPE // 2
    locals_[4].wait()
    key_swap = jnp.concatenate([key_raw[half:], key_raw[:half]], axis=0)
    key_rotary = key_raw * key_tab[0:ROPE, :] + key_swap * key_tab[ROPE : 2 * ROPE, :]
    latbuf[me, mine, rows : rows + ROPE, 0:rows] = key_rotary.astype(BF16)

    def lat_part(slot, t):
        return latbuf.at[slot, t, pl.ds(0, rows)]

    def lat_copy(slot, k):
        return pltpu.make_async_remote_copy(
            src_ref=lat_part(slot, mine),
            dst_ref=lat_part(slot, mine),
            send_sem=lat_send.at[slot, k],
            recv_sem=lat_recv.at[slot, mine],
            device_id={"tp": (mine + k) % tp},
            device_id_type=MESH,
        )

    def lat_wait(slot):
        for k in range(1, tp):
            t = (mine + k) % tp
            pltpu.make_async_copy(lat_part(slot, t), lat_part(slot, t), lat_recv.at[slot, t]).wait()

    def sp_copy(target):
        return pltpu.make_async_remote_copy(
            src_ref=latbuf.at[me, mine],
            dst_ref=latbuf.at[me, mine],
            send_sem=sp_send.at[target],
            recv_sem=lat_recv.at[me, mine],
            device_id={"sp": target},
            device_id_type=MESH,
        )

    def sp_start(target, carry):
        sp_copy(target).start()
        return carry

    lax.fori_loop(me + 1, sp, sp_start, 0)
    for k in range(1, tp):
        lat_copy(me, k).start()

    qlat[mine] = dot_nt(own, query_down[...]).astype(BF16)

    def q_copy(k):
        return pltpu.make_async_remote_copy(
            src_ref=qlat.at[mine],
            dst_ref=qlat.at[mine],
            send_sem=q_send.at[k],
            recv_sem=q_recv.at[mine],
            device_id={"tp": (mine + k) % tp},
            device_id_type=MESH,
        )

    for k in range(1, tp):
        q_copy(k).start()

    @pl.when(me == 0)
    def _():
        normed[pl.ds(0, HALO), :] = jnp.zeros((HALO, normed.shape[1]), BF16)

    @pl.when(me > 0)
    def _():
        halo_copy.wait_recv()
        normed[pl.ds(0, HALO), :] = normalized(halo[...], pre_gain[...]).astype(BF16)

    aligned = depth % 128 == 0

    def gate_step(i, slot, first=False):
        columns = pl.ds(pl.multiple_of(slot * depth, depth), depth)
        value = dot(normed[:, columns], wbuf[i, sp_row(slot), :])
        if first:
            acc[i] = value
        else:
            acc[i] += value

    if aligned:
        for i in range(3):
            gate_step(i, me, True)

    w_wait(late, pair)
    up(late, pair)
    down(late, pair)

    def forward(k):
        slot = me - k
        pltpu.make_async_copy(
            latbuf.at[slot, mine], latbuf.at[slot, mine], lat_recv.at[slot, mine]
        ).wait()
        for t in range(1, tp):
            lat_copy(slot, t).start()

    def forward_some(first, last):
        def one(k, carry):
            forward(k)
            return carry

        lax.fori_loop(first, jnp.minimum(last, me) + 1, one, 0)

    group = 2 * inner

    def line_step(d, carry):
        @pl.when(d > 1)
        def _():
            forward_some(group * (d - 2) + 1, group * (d - 1))

        for u in range(late + 1):

            @pl.when(zi - d >= 0)
            def _():
                slot = me - d * inner
                w_wait(u, slot)
                up(u, slot)
                if u < late:
                    w_copy(u, slot, 2).start()
                else:
                    w_wait(u, pair - d * inner)
                    up(u, pair - d * inner)

            @pl.when(zi + d <= lines - 1)
            def _():
                slot = me + d * inner
                w_wait(u, slot)
                down(u, slot)
                if u < late:
                    w_copy(u, slot, 2).start()
                else:
                    w_wait(u, pair + d * inner)
                    down(u, pair + d * inner)

        if aligned:

            @pl.when(zi - d >= 0)
            def _():
                for i in range(3):
                    gate_step(i, me - d * inner)

            @pl.when(zi + d <= lines - 1)
            def _():
                for i in range(3):
                    gate_step(i, me + d * inner)

        return carry

    lax.fori_loop(1, lines, line_step, 0)

    forward_some(group * (lines - 2) + 1, sp - 1)

    lane = lax.broadcasted_iota(jnp.int32, (rows, heads * NOPE), 1)
    width = heads * ROPE
    for k in range(1, tp):
        t = (mine + k) % tp
        pltpu.make_async_copy(qlat.at[t], qlat.at[t], q_recv.at[t]).wait()
    query_latent = jnp.concatenate([qlat[t].astype(F32) for t in range(tp)], axis=1)
    query_normed = normalized(query_latent, query_gain[...]).astype(BF16)
    query_nope = dot(query_normed, query_up[...])
    turned = dot_nt(query_normed, query_rotary[...])
    locals_[3].wait()
    turned = (turned * tab[:, :width] + swapped(turned) * tab[:, width : 2 * width]).astype(BF16)
    for h in range(heads):
        qnope[h] = jnp.where(lane // NOPE == h, query_nope, 0.0).astype(BF16)
        qturn[h] = turned[:, h * ROPE : (h + 1) * ROPE]

    factor = (NOPE + ROPE) ** (-0.5)

    def keys_of(slot):
        lat_wait(slot)
        latent = jnp.concatenate([latbuf[slot, t, 0:rows, 0:kl] for t in range(tp)], axis=1)
        latent_normed = normalized(latent, latent_gain[...]).astype(BF16)
        key_nope = dot(latent_normed, key_up[...]).astype(BF16)
        values = dot(latent_normed, value_up[...]).astype(BF16)
        return key_nope, values, latbuf[slot, mine, rows : rows + ROPE, 0:rows]

    def scores_of(h, key_nope, turned_keys):
        return (dot_nt(qnope[h], key_nope) + dot(qturn[h], turned_keys)) * factor

    key_nope, values, turned_keys = keys_of(me)
    row_id = lax.broadcasted_iota(jnp.int32, (rows, rows), 0)
    key_id = lax.broadcasted_iota(jnp.int32, (rows, rows), 1)
    for h in range(heads):
        scores = jnp.where(key_id <= row_id, scores_of(h, key_nope, turned_keys), -1e30)
        top = jnp.max(scores, axis=-1, keepdims=True)
        weights = jnp.where(key_id <= row_id, jnp.exp(scores - top), 0.0)
        best[h] = top
        total[h] = jnp.sum(weights, axis=-1, keepdims=True)
        weighted[h] = dot(weights.astype(BF16), values)

    def attend(k, carry):
        key_nope, values, turned_keys = keys_of(me - k)
        for h in range(heads):
            scores = scores_of(h, key_nope, turned_keys)
            old = best[h]
            top = jnp.maximum(old, jnp.max(scores, axis=-1, keepdims=True))
            weights = jnp.exp(scores - top)
            shrink = jnp.exp(old - top)
            best[h] = top
            total[h] = total[h] * shrink + jnp.sum(weights, axis=-1, keepdims=True)
            weighted[h] = weighted[h] * shrink + dot(weights.astype(BF16), values)
        return carry

    lax.fori_loop(1, me + 1, attend, 0)
    value_lane = lax.broadcasted_iota(jnp.int32, (rows, heads * VDIM), 1)
    heads_mixed = jnp.zeros((rows, heads * VDIM), F32)
    for h in range(heads):
        logsum = best[h] + jnp.log(total[h])
        row_logsum[h : h + 1, :] = jnp.transpose(jnp.broadcast_to(logsum, (rows, rows)))[0:1, :]
        heads_mixed = jnp.where(value_lane // VDIM == h, weighted[h] / total[h], heads_mixed)
    locals_[5].wait()
    proj[...] = dot(heads_mixed.astype(BF16), wheads[...])

    def pair_slot(slot):
        for u in range(late):
            w_wait(u, slot)
        if aligned:
            for i in range(3):
                gate_step(i, slot)

    pair_slot(pair)

    def pair_step(d, carry):
        @pl.when(zi - d >= 0)
        def _():
            pair_slot(pair - d * inner)

        @pl.when(zi + d <= lines - 1)
        def _():
            pair_slot(pair + d * inner)

        return carry

    lax.fori_loop(1, lines, pair_step, 0)
    if not aligned:
        for i in range(3):
            acc[i] = dot(normed[...], wbuf[i])

    prod[...] = (acc[1] * acc[2]).astype(BF16).astype(F32)
    convolved = prod[pl.ds(HALO - TAPS + 1, rows), :] * conv_taps[0:1, :]
    for k in range(1, TAPS):
        convolved = convolved + prod[pl.ds(HALO - TAPS + 1 + k, rows), :] * conv_taps[k : k + 1, :]
    convm[...] = (acc[0, pl.ds(HALO, rows), :] * convolved).astype(BF16)

    locals_[6].wait()
    part = rows // tp

    def share(target):
        where = pl.ds(pl.multiple_of(target * part, part), part)
        return proj[where, :] + dot(convm[where, :], wout[...])

    def rs_copy(k):
        return pltpu.make_async_remote_copy(
            src_ref=outbuf.at[k],
            dst_ref=rsbuf.at[mine],
            send_sem=rs_send.at[k],
            recv_sem=rs_recv.at[mine],
            device_id={"tp": (mine + k) % tp},
            device_id_type=MESH,
        )

    order = sorted(range(1, tp), key=lambda k: abs(k - tp // 2))
    for k in order:
        outbuf[k] = share((mine + k) % tp).astype(BF16)
        rs_copy(k).start()
    result = share(mine)
    for k in range(1, tp):
        other = (mine + k) % tp
        pltpu.make_async_copy(rsbuf.at[other], rsbuf.at[other], rs_recv.at[other]).wait()
        result = result + rsbuf[other].astype(F32)
    mixed[...] = normalized(result, post_gain[...]).astype(BF16)

    for k in range(1, tp):
        rs_copy(k).wait_send()
        q_copy(k).wait_send()

    def lat_end(slot, carry):
        for k in range(1, tp):
            lat_copy(slot, k).wait_send()
        return carry

    lax.fori_loop(0, me + 1, lat_end, 0)

    @pl.when(me < sp - 1)
    def _():
        halo_copy.wait_send()

    def sp_end(target, carry):
        sp_copy(target).wait_send()
        return carry

    lax.fori_loop(me + 1, sp, sp_end, 0)

    def line_ends(u, z, slot):
        @pl.when((z <= zi) & (zi < lines - 1))
        def _():
            w_copy(u, slot, 0).wait_send()

        @pl.when((z >= zi) & (zi > 0))
        def _():
            w_copy(u, slot, 1).wait_send()

    def w_end(z, carry):
        slot = z * inner + xi
        for u in range(late):
            w_copy(u, slot, 2).wait_send()
            line_ends(u, z, slot)
        for x in range(inner):
            line_ends(late, z, z * inner + x)
        return carry

    lax.fori_loop(0, lines, w_end, 0)
    w_copy(late, me, 2).wait_send()


def w_units(channels):
    half = channels // 2
    return (0, 0, channels), (1, 0, channels), (2, 0, half), (2, half, half)


def rope_tables(blocks, rows, heads):
    half = ROPE // 2
    frequency = np.float32(rope_theta) ** (-np.arange(half, dtype=np.float32) / np.float32(half))
    positions = np.arange(blocks * rows, dtype=np.float32)
    angles = positions[:, None] * frequency.astype(np.float32)
    cosine = np.concatenate([np.cos(angles)] * 2, 1)
    sine = np.concatenate([-np.sin(angles), np.sin(angles)], 1)
    table = np.concatenate([cosine] * heads + [sine] * heads, 1).astype(np.float32)
    keys = np.concatenate([cosine, sine], 1).astype(np.float32).reshape(blocks, rows, 2 * ROPE)
    return table.reshape(blocks, rows, -1), keys.transpose(0, 2, 1).copy()


def solution(mesh):
    sp, tp = mesh.shape["sp"], mesh.shape["tp"]
    inner = 2

    def local(
        tokens, pre_gain, outer_gate, inner_gate, conv_input, conv_taps, query_down, latent_down,
        rotary_down, query_gain, latent_gain, query_up, query_rotary, key_up, value_up,
        conv_output, heads_output, post_gain,
    ):
        rows, model = tokens.shape
        depth, channels = outer_gate.shape
        heads = query_up.shape[1] // NOPE
        ql, kl = query_down.shape[1], latent_down.shape[1]
        units = len(w_units(channels))
        part = rows // tp
        table, key_table = map(jnp.asarray, rope_tables(sp, rows, heads))
        vm = pl.BlockSpec(memory_space=pltpu.VMEM)
        hbm = pl.BlockSpec(memory_space=pl.ANY)
        dma = pltpu.SemaphoreType.DMA
        return pl.pallas_call(
            functools.partial(kernel, sp, tp, inner),
            out_shape=(
                jax.ShapeDtypeStruct((part, model), BF16),
                jax.ShapeDtypeStruct((heads, rows), F32),
            ),
            in_specs=[
                vm, vm, hbm, hbm, hbm, vm, vm, vm, vm, vm, vm, vm, vm, vm, vm, hbm, hbm, vm, hbm, hbm,
            ],
            out_specs=(vm, vm),
            scratch_shapes=[
                pltpu.VMEM((3, sp * depth, channels), BF16),
                pltpu.VMEM((rows + HALO, model), BF16),
                pltpu.VMEM((HALO, model), BF16),
                pltpu.VMEM((3, rows + HALO, channels), F32),
                pltpu.VMEM((rows + HALO, channels), F32),
                pltpu.VMEM((tp, rows, ql), BF16),
                pltpu.VMEM((sp, tp, rows + ROPE, max(kl, rows)), BF16),
                pltpu.VMEM((heads, rows, heads * NOPE), BF16),
                pltpu.VMEM((heads, rows, ROPE), BF16),
                pltpu.VMEM((heads, rows, 1), F32),
                pltpu.VMEM((heads, rows, 1), F32),
                pltpu.VMEM((heads, rows, heads * VDIM), F32),
                pltpu.VMEM((rows, model), F32),
                pltpu.VMEM((rows, channels), BF16),
                pltpu.VMEM((tp, part, model), BF16),
                pltpu.VMEM((tp, part, model), BF16),
                pltpu.VMEM(conv_output.shape, BF16),
                pltpu.VMEM(heads_output.shape, BF16),
                pltpu.VMEM((rows, 2 * heads * ROPE), F32),
                pltpu.VMEM((2 * ROPE, rows), F32),
                dma((7,)),
                dma((units, sp)),
                dma((3, units, sp)),
                dma((2,)),
                dma((tp,)),
                dma((tp,)),
                dma((sp, tp)),
                dma((sp, tp)),
                dma((sp,)),
                dma((tp,)),
                dma((tp,)),
            ],
            compiler_params=pltpu.CompilerParams(collective_id=0, has_side_effects=True),
        )(
            tokens, pre_gain.reshape(1, -1), outer_gate, inner_gate, conv_input, conv_taps,
            query_down.T, latent_down, rotary_down.T, query_gain.reshape(1, -1),
            latent_gain.reshape(1, -1), query_up, query_rotary.T, key_up, value_up,
            conv_output, heads_output, post_gain.reshape(1, -1), table, key_table,
        )

    in_specs = (
        P("sp", None), P(), P("sp", "tp"), P("sp", "tp"), P("sp", "tp"), P(None, "tp"),
        P(None, "tp"), P(None, "tp"), P(), P(), P(), P(None, "tp"), P(None, "tp"),
        P(None, "tp"), P(None, "tp"), P("tp", None), P("tp", None), P(),
    )
    out_specs = (P(("sp", "tp"), None), P("tp", "sp"))
    return jax.shard_map(local, mesh=mesh, in_specs=in_specs, out_specs=out_specs, check_vma=False)
```

time: 72.3 us -> 65.4 us (0.905)
  local copies, waits for them, and re-layouts: 8.38 us -> 3.39 us
  Pallas kernels: 63.1 us -> 61 us
    unnamed x11 -> x6, local copies, waits for them, and re-layouts: 7.71 us -> 2.81 us
    pallas_call x1, Pallas kernels: 63.1 us -> 61 us  [local(): pl.pallas_call(functools.partial(kernel, sp, tp, inner), out_shape=(jax.S...]
where the time goes in v2:
time: 65.4 us; the launch traced here: 65.1 us
  Pallas kernels  61 us (93%)
  local copies, waits for them, and re-layouts  3.39 us (5%)
  between operations  0.66 us (1%)
    pallas_call x1, Pallas kernels, local(): pl.pallas_call(functools.partial(kernel, sp, tp, inner), out_shape=(jax.S...  61 us
    unnamed x6, local copies, waits for them, and re-layouts  2.81 us

profile of v2, /device:TPU:27, one launch (start us, length us, event | category | flops | bytes accessed | tf_op | source)
XLA Modules:
  0.0 65.1 jit_solution(16527292934852400669)
XLA Ops:
  0.6 0.0 copy-start
  0.6 0.7 %copy-done = f32[768]{0:T(1024)S(1)} copy-done((f32[768]{0:T(1024)S(1)}, f32[768]{0:T(1024)}, u32[]{:S(2)}) %copy-start) | copy-done | bytes 3096
  1.3 0.6 reshape.17.query_gain
  1.9 61.0 %shard_map.203 = (bf16[32,2048]{1,0:T(8,128)(2,1)}, f32[2,128]{1,0:T(2,128)}) custom-call(bf16[128,2048]{1,0:T(8,128)(2,1)} %tokens.1, f32[1,2048]{1,0:T(1,128)} %bitcast.9, bf16[256,256]{1,0:T(8,128)(2,1)} %outer_gate.1, bf16[256,256]{1,0:T(8,128)(2,1)} %inner_gate.1, bf16[256,256]{1,0:T(8,128)(2,1)} %conv_input.1, f32[3,256]{1,0:T(4,128)} %conv_taps.1, ...), custom_call_target="tpu_custom_call" | custom-call | tf_op jit(solution)/shard_map/pallas_call | solution.py:506
  62.9 0.0 copy-start.1
  62.9 1.6 %copy.24 = bf16[32,2048]{1,0:T(8,128)(2,1)} copy(bf16[32,2048]{1,0:T(8,128)(2,1)} %get-tuple-element.4) | data formatting | bytes 262144
  64.5 0.0 copy-done.1
  64.5 0.6 copy.25
Async XLA Ops:
  0.6 0.7 %copy-start = (f32[768]{0:T(1024)S(1)}, f32[768]{0:T(1024)}, u32[]{:S(2)}) copy-start(f32[768]{0:T(1024)} %param.29) | copy-start | bytes 9220
  62.9 1.6 %copy-start.1 = (f32[2,128]{1,0:T(2,128)S(1)}, f32[2,128]{1,0:T(2,128)}, u32[]{:S(2)}) copy-start(f32[2,128]{1,0:T(2,128)} %get-tuple-element.5) | copy-start | bytes 3076

commit v3 on v2

--- a/solution.py
+++ b/solution.py
@@ -256,53 +256,6 @@
 
     group = 2 * inner
 
-    def line_step(d, carry):
-        @pl.when(d > 1)
-        def _():
-            forward_some(group * (d - 2) + 1, group * (d - 1))
-
-        for u in range(late + 1):
-
-            @pl.when(zi - d >= 0)
-            def _():
-                slot = me - d * inner
-                w_wait(u, slot)
-                up(u, slot)
-                if u < late:
-                    w_copy(u, slot, 2).start()
-                else:
-                    w_wait(u, pair - d * inner)
-                    up(u, pair - d * inner)
-
-            @pl.when(zi + d <= lines - 1)
-            def _():
-                slot = me + d * inner
-                w_wait(u, slot)
-                down(u, slot)
-                if u < late:
-                    w_copy(u, slot, 2).start()
-                else:
-                    w_wait(u, pair + d * inner)
-                    down(u, pair + d * inner)
-
-        if aligned:
-
-            @pl.when(zi - d >= 0)
-            def _():
-                for i in range(3):
-                    gate_step(i, me - d * inner)
-
-            @pl.when(zi + d <= lines - 1)
-            def _():
-                for i in range(3):
-                    gate_step(i, me + d * inner)
-
-        return carry
-
-    lax.fori_loop(1, lines, line_step, 0)
-
-    forward_some(group * (lines - 2) + 1, sp - 1)
-
     lane = lax.broadcasted_iota(jnp.int32, (rows, heads * NOPE), 1)
     width = heads * ROPE
     for k in range(1, tp):
@@ -355,7 +308,83 @@
             weighted[h] = weighted[h] * shrink + dot(weights.astype(BF16), values)
         return carry
 
-    lax.fori_loop(1, me + 1, attend, 0)
+    def pair_slot(slot):
+        for u in range(late):
+            w_wait(u, slot)
+        if aligned:
+            for i in range(3):
+                gate_step(i, slot)
+
+    def attend_some(first, last):
+        lax.fori_loop(first, jnp.minimum(last, me) + 1, attend, 0)
+
+    def pair_at(d):
+        @pl.when(d == 0)
+        def _():
+            pair_slot(pair)
+
+        @pl.when((d > 0) & (zi - d >= 0))
+        def _():
+            pair_slot(pair - d * inner)
+
+        @pl.when((d > 0) & (zi + d <= lines - 1))
+        def _():
+            pair_slot(pair + d * inner)
+
+    def line_step(d, carry):
+        @pl.when(d > 1)
+        def _():
+            forward_some(group * (d - 2) + 1, group * (d - 1))
+
+        for u in range(late + 1):
+            if u == 2:
+
+                @pl.when(d > 1)
+                def _():
+                    attend_some(group * (d - 2) + 1, group * (d - 1))
+                    pair_at(d - 2)
+
+            @pl.when(zi - d >= 0)
+            def _():
+                slot = me - d * inner
+                w_wait(u, slot)
+                up(u, slot)
+                if u < late:
+                    w_copy(u, slot, 2).start()
+                else:
+                    w_wait(u, pair - d * inner)
+                    up(u, pair - d * inner)
+
+            @pl.when(zi + d <= lines - 1)
+            def _():
+                slot = me + d * inner
+                w_wait(u, slot)
+                down(u, slot)
+                if u < late:
+                    w_copy(u, slot, 2).start()
+                else:
+                    w_wait(u, pair + d * inner)
+                    down(u, pair + d * inner)
+
+        if aligned:
+
+            @pl.when(zi - d >= 0)
+            def _():
+                for i in range(3):
+                    gate_step(i, me - d * inner)
+
+            @pl.when(zi + d <= lines - 1)
+            def _():
+                for i in range(3):
+                    gate_step(i, me + d * inner)
+
+        return carry
+
+    lax.fori_loop(1, lines, line_step, 0)
+
+    forward_some(group * (lines - 2) + 1, sp - 1)
+
+    attend_some(group * (lines - 2) + 1, sp - 1)
     value_lane = lax.broadcasted_iota(jnp.int32, (rows, heads * VDIM), 1)
     heads_mixed = jnp.zeros((rows, heads * VDIM), F32)
     for h in range(heads):
@@ -365,27 +394,11 @@
     locals_[5].wait()
     proj[...] = dot(heads_mixed.astype(BF16), wheads[...])
 
-    def pair_slot(slot):
-        for u in range(late):
-            w_wait(u, slot)
-        if aligned:
-            for i in range(3):
-                gate_step(i, slot)
-
-    pair_slot(pair)
-
-    def pair_step(d, carry):
-        @pl.when(zi - d >= 0)
-        def _():
-            pair_slot(pair - d * inner)
-
-        @pl.when(zi + d <= lines - 1)
-        def _():
-            pair_slot(pair + d * inner)
-
-        return carry
-
-    lax.fori_loop(1, lines, pair_step, 0)
+    def pair_end(d, carry):
+        pair_at(d)
+        return carry
+
+    lax.fori_loop(max(0, lines - 2), lines, pair_end, 0)
     if not aligned:
         for i in range(3):
             acc[i] = dot(normed[...], wbuf[i])

time: 65.4 us -> 58.2 us (0.89)
  the two profiles are of different devices: /device:TPU:27 before, /device:TPU:25 now
where the time goes in v3:
time: 58.2 us; the launch traced here: 58 us
  Pallas kernels  54 us (93%)
  local copies, waits for them, and re-layouts  3.39 us (6%)
  between operations  0.66 us (1%)
    pallas_call x1, Pallas kernels, local(): pl.pallas_call(functools.partial(kernel, sp, tp, inner), out_shape=(jax.S...  54 us
    unnamed x6, local copies, waits for them, and re-layouts  2.81 us

profile of v3, /device:TPU:25, one launch (start us, length us, event | category | flops | bytes accessed | tf_op | source)
XLA Modules:
  0.0 58.0 jit_solution(6374165950538792521)
XLA Ops:
  0.6 0.0 copy-start
  0.6 0.7 %copy-done = f32[768]{0:T(1024)S(1)} copy-done((f32[768]{0:T(1024)S(1)}, f32[768]{0:T(1024)}, u32[]{:S(2)}) %copy-start) | copy-done | bytes 3096
  1.3 0.6 reshape.17.query_gain
  1.9 54.0 %shard_map.203 = (bf16[32,2048]{1,0:T(8,128)(2,1)}, f32[2,128]{1,0:T(2,128)}) custom-call(bf16[128,2048]{1,0:T(8,128)(2,1)} %tokens.1, f32[1,2048]{1,0:T(1,128)} %bitcast.9, bf16[256,256]{1,0:T(8,128)(2,1)} %outer_gate.1, bf16[256,256]{1,0:T(8,128)(2,1)} %inner_gate.1, bf16[256,256]{1,0:T(8,128)(2,1)} %conv_input.1, f32[3,256]{1,0:T(4,128)} %conv_taps.1, ...), custom_call_target="tpu_custom_call" | custom-call | tf_op jit(solution)/shard_map/pallas_call | solution.py:519
  55.9 0.0 copy-start.1
  55.9 1.6 %copy.24 = bf16[32,2048]{1,0:T(8,128)(2,1)} copy(bf16[32,2048]{1,0:T(8,128)(2,1)} %get-tuple-element.4) | data formatting | bytes 262144
  57.5 0.0 copy-done.1
  57.5 0.6 copy.25
Async XLA Ops:
  0.6 0.7 %copy-start = (f32[768]{0:T(1024)S(1)}, f32[768]{0:T(1024)}, u32[]{:S(2)}) copy-start(f32[768]{0:T(1024)} %param.29) | copy-start | bytes 9220
  55.9 1.6 %copy-start.1 = (f32[2,128]{1,0:T(2,128)S(1)}, f32[2,128]{1,0:T(2,128)}, u32[]{:S(2)}) copy-start(f32[2,128]{1,0:T(2,128)} %get-tuple-element.5) | copy-start | bytes 3076
